TPU v7x, 32 devices: a whole 2x2x4 slice. The times are simulated.
32 devices in a mesh: sp: 4 (over z), fs: 4 (over y, x), tp: 2 (over core).
Axes of the slice: x: 2, y: 2, z: 4, core: 2. Of those that a mesh axis runs over, the one named last changes fastest.
Arguments:
- queries: bfloat16 [4, 1024, 512], P('fs', 'sp', 'tp'), may hold values from -60 to 60
- keys: bfloat16 [4, 1024, 256], P('fs', 'sp', 'tp'), may hold values from -4.5 to 4.5
- values: bfloat16 [4, 1024, 256], P('fs', 'sp', 'tp'), may hold values from -6 to 6
- forget_cache: float32 [4, 1024, 8], P('fs', 'sp', 'tp'), may hold values from -128 to 0, as said below
- fox_gain: float32 [512], P('tp'), may hold values from 0.1 to 1.9
- receptance: bfloat16 [4, 1024, 512], P('fs', 'sp', 'tp'), may hold values from -6 to 6
- lin_keys: bfloat16 [4, 1024, 512], P('fs', 'sp', 'tp'), may hold values from -6 to 6
- lin_values: bfloat16 [4, 1024, 512], P('fs', 'sp', 'tp'), may hold values from -6 to 6
- learn_logit: bfloat16 [4, 1024, 512], P('fs', 'sp', 'tp'), may hold values from -12 to 4
- decay_log: float32 [4, 1024, 512], P('fs', 'sp', 'tp'), may hold values from -16 to 0
- lin_gain: float32 [512], P('tp'), may hold values from 0.1 to 1.9
- out_fox_weight: bfloat16 [512, 2048], P('tp', 'fs'), may hold values from -0.1875 to 0.1875
- out_lin_weight: bfloat16 [512, 2048], P('tp', 'fs'), may hold values from -0.1875 to 0.1875
Outputs:
- mixed: bfloat16 [4, 1024, 2048], P('fs', ('sp', 'tp'))
Inputs may be any that keep to these rules, and one draw needn't show every extreme that they name: `forget_cache`: Non-increasing along the positions of each sequence and head.
All inputs are finite; a program needn't handle non-finite values.
Results may differ from a plain program's by a relative error of at most 0.017.
Values may be sent and summed in bfloat16 or wider, within the bound.
A program may use at most 64 MiB of HBM per device.

v0:
```python
import math
import jax
import jax.numpy as jnp
from jax import lax
from jax.sharding import PartitionSpec as P

HEAD = 64
SPAN = 64
HIGHEST = lax.Precision.HIGHEST
NORM_EPS = 1e-06


def carried_in(shard, axis, join, neutral):
    place = lax.axis_index(axis)
    gathered = jax.tree.map(
        lambda a, kind: lax.all_gather(a.astype(kind), axis), shard, (jnp.bfloat16, jnp.bfloat16)
    )
    state = jax.tree.map(lambda a, e: jnp.zeros_like(a) + jnp.asarray(e, a.dtype), shard, neutral)

    def one(lap, state):
        return join(
            state,
            jax.tree.map(
                lambda a, own: lax.dynamic_index_in_dim(a, lap, 0, False).astype(own.dtype),
                gathered,
                shard,
            ),
        )

    return lax.fori_loop(0, place, one, state)


def round_half(tensor):
    return lax.optimization_barrier(tensor.astype(jnp.bfloat16)).astype(jnp.float32)


def forget_attention(query_rows, key_rows, value_rows, forget_rows, fox_gain):
    row_count = query_rows.shape[0]
    head_count = query_rows.shape[1] // HEAD
    kv_count = key_rows.shape[1] // HEAD
    group_size = head_count // kv_count
    score_scale = HEAD ** (-0.5)
    own_first = lax.axis_index("sp") * row_count
    forget_all = lax.all_gather(forget_rows, "sp", axis=0, tiled=True)
    forget_own = forget_rows.reshape(row_count, kv_count, group_size)
    query_heads = query_rows.reshape(row_count, kv_count, group_size, HEAD)
    query_pos = own_first + jnp.arange(row_count, dtype=jnp.int32)
    start_state = (
        jnp.full((row_count, kv_count, group_size), -1e30, jnp.float32),
        jnp.zeros((row_count, kv_count, group_size), jnp.float32),
        jnp.zeros((row_count, kv_count, group_size, HEAD), jnp.float32),
    )
    key_piece = lax.all_gather(key_rows, "sp", axis=0, tiled=True)
    value_piece = lax.all_gather(value_rows, "sp", axis=0, tiled=True)
    piece_rows = key_piece.shape[0]
    block_rows = math.gcd(piece_rows, 512)

    def attend(state):

        def one_block(block_index, inner):
            running_max, totals, weighted = inner
            local_first = (block_index * block_rows).astype(jnp.int32)
            key_block = lax.dynamic_slice_in_dim(key_piece, local_first, block_rows, 0).reshape(
                block_rows, kv_count, HEAD
            )
            value_block = lax.dynamic_slice_in_dim(value_piece, local_first, block_rows, 0).reshape(
                block_rows, kv_count, HEAD
            )
            forget_block = lax.dynamic_slice_in_dim(forget_all, local_first, block_rows, 0).reshape(
                block_rows, kv_count, group_size
            )
            key_pos = local_first + jnp.arange(block_rows, dtype=jnp.int32)
            allowed = (key_pos[None, :] <= query_pos[:, None])[:, None, None, :]
            scores = jnp.einsum(
                "tkgd,skd->tkgs", query_heads, key_block, preferred_element_type=jnp.float32
            )
            scores = (
                scores * score_scale
                + forget_own[..., None]
                - jnp.transpose(forget_block, (1, 2, 0))[None]
            )
            scores = jnp.where(allowed, scores, -1e30)
            new_max = jnp.maximum(running_max, jnp.max(scores, axis=-1))
            rescale = jnp.exp(running_max - new_max)
            weights = jnp.where(allowed, jnp.exp(scores - new_max[..., None]), 0.0)
            totals = totals * rescale + jnp.sum(weights, axis=-1)
            update = jnp.einsum(
                "tkgs,skd->tkgd",
                weights.astype(jnp.bfloat16),
                value_block,
                preferred_element_type=jnp.float32,
            )
            weighted = weighted * rescale[..., None] + update
            return (new_max, totals, weighted)

        return lax.fori_loop(0, piece_rows // block_rows, one_block, state)

    def keep_state(running_state):
        return running_state

    running_max, totals, weighted = lax.cond(
        jnp.int32(0) < own_first + row_count, attend, keep_state, start_state
    )
    attended = (weighted / totals[..., None]).reshape(row_count, head_count, HEAD)
    normed = attended * lax.rsqrt(jnp.mean(attended * attended, axis=-1, keepdims=True) + NORM_EPS)
    return (
        (normed * fox_gain.reshape(head_count, HEAD))
        .reshape(row_count, head_count * HEAD)
        .astype(jnp.bfloat16)
    )


def product(left, right, form):
    return jnp.einsum(form, left, right, precision=HIGHEST)


def delta_attention(recept_rows, key_rows, value_rows, learn_rows, decay_rows, lin_gain):
    row_count = recept_rows.shape[0]
    head_count = recept_rows.shape[1] // HEAD
    span_count = row_count // SPAN

    def arrange(tensor):
        return jnp.transpose(
            tensor.astype(jnp.float32).reshape(span_count, SPAN, head_count, HEAD), (0, 2, 1, 3)
        )

    recept = arrange(recept_rows)
    key_float = arrange(key_rows)
    value_float = arrange(value_rows)
    learn_rate = jax.nn.sigmoid(arrange(learn_rows))
    unit_keys = key_float * lax.rsqrt(
        jnp.sum(key_float * key_float, axis=-1, keepdims=True) + NORM_EPS
    )
    log_decay = -jnp.exp(arrange(decay_rows))
    strict_lower = jnp.tril(jnp.ones((SPAN, SPAN), jnp.float32), -1)
    with_diagonal = jnp.tril(jnp.ones((SPAN, SPAN), jnp.float32))
    identity_head = jnp.broadcast_to(jnp.eye(HEAD, dtype=jnp.float32), (head_count, HEAD, HEAD))
    identity_span = jnp.broadcast_to(jnp.eye(SPAN, dtype=jnp.float32), (head_count, SPAN, SPAN))
    zero_state = jnp.zeros((head_count, HEAD, HEAD), jnp.float32)

    def one_span(state, inputs):
        recept_t, key_t, value_t, unit_t, rate_t, fall_t = inputs
        inclusive = jnp.cumsum(fall_t, axis=1)
        grown = jnp.exp(inclusive)
        shrunk = jnp.exp(-inclusive)
        erase_in = -unit_t * jnp.exp(inclusive - fall_t)
        read_in = recept_t * grown
        erase_out = unit_t * rate_t * shrunk
        write_out = key_t * shrunk
        padded_values = jnp.concatenate([value_t, jnp.zeros_like(value_t)], axis=-1)
        mix_erase = product(erase_in, erase_out, "hid,hjd->hij") * strict_lower
        mix_write = product(erase_in, write_out, "hid,hjd->hij") * strict_lower
        read_erase = product(read_in, erase_out, "hid,hjd->hij") * with_diagonal
        read_write = product(read_in, write_out, "hid,hjd->hij") * with_diagonal
        right_side = product(erase_in, state, "hid,hrd->hir") + product(
            mix_write, padded_values, "hij,hjr->hir"
        )
        erased = jax.scipy.linalg.solve_triangular(
            identity_span - mix_erase, right_side, lower=True, unit_diagonal=True
        )
        outputs = (
            product(read_in, state, "hid,hrd->hir")
            + product(read_erase, erased, "hij,hjr->hir")
            + product(read_write, padded_values, "hij,hjr->hir")
        )
        final_grow = grown[:, -1, :]
        state = (
            state * final_grow[:, None, :]
            + product(erased, erase_out * final_grow[:, None, :], "hlr,hld->hrd")
            + product(padded_values, write_out * final_grow[:, None, :], "hlr,hld->hrd")
        )
        return (state, outputs)

    start_state = jnp.concatenate([zero_state, identity_head], axis=1)
    final_state, outputs = lax.scan(
        one_span, start_state, (recept, key_float, value_float, unit_keys, learn_rate, log_decay)
    )
    local_read = outputs[..., :HEAD]
    carried_read = outputs[..., HEAD:]

    def chain(earlier, later):
        return (
            product(earlier[0], later[0], "hij,hjk->hik"),
            product(earlier[1], later[0], "hij,hjk->hik") + later[1],
        )

    entry_map, entry_state = carried_in(
        (final_state[:, HEAD:], final_state[:, :HEAD]), "sp", chain, (identity_head, zero_state)
    )
    readout = local_read + jnp.einsum(
        "hvk,nhtk->nhtv", entry_state, carried_read, precision=HIGHEST
    )
    readout = jnp.transpose(readout, (0, 2, 1, 3)).reshape(row_count, head_count, HEAD)
    centred = readout - jnp.mean(readout, axis=-1, keepdims=True)
    normed = centred * lax.rsqrt(jnp.mean(centred * centred, axis=-1, keepdims=True) + HEAD * 1e-05)
    return (
        (normed * lin_gain.reshape(head_count, HEAD))
        .reshape(row_count, head_count * HEAD)
        .astype(jnp.bfloat16)
    )


def shards(
    queries,
    keys,
    values,
    forget_cache,
    fox_gain,
    receptance,
    lin_keys,
    lin_values,
    learn_logit,
    decay_log,
    lin_gain,
    out_fox_weight,
    out_lin_weight,
):
    fox_out = forget_attention(queries[0], keys[0], values[0], forget_cache[0], fox_gain)
    lin_out = delta_attention(
        receptance[0], lin_keys[0], lin_values[0], learn_logit[0], decay_log[0], lin_gain
    )
    fox_weight, lin_weight = (
        lax.all_gather(out_fox_weight, "fs", axis=1, tiled=True),
        lax.all_gather(out_lin_weight, "fs", axis=1, tiled=True),
    )
    partial_value = jnp.dot(fox_out, fox_weight, preferred_element_type=jnp.float32)
    partial_value = partial_value + jnp.dot(lin_out, lin_weight, preferred_element_type=jnp.float32)
    summed = lax.psum_scatter(
        round_half(partial_value).astype(jnp.bfloat16), "tp", scatter_dimension=0, tiled=True
    )
    return summed[None]


def solution(mesh):
    return jax.shard_map(
        shards,
        mesh=mesh,
        in_specs=(
            P("fs", "sp", "tp"),
            P("fs", "sp", "tp"),
            P("fs", "sp", "tp"),
            P("fs", "sp", "tp"),
            P("tp"),
            P("fs", "sp", "tp"),
            P("fs", "sp", "tp"),
            P("fs", "sp", "tp"),
            P("fs", "sp", "tp"),
            P("fs", "sp", "tp"),
            P("tp"),
            P("tp", "fs"),
            P("tp", "fs"),
        ),
        out_specs=P("fs", ("sp", "tp"), None),
        check_vma=False,
    )
```

profile of v0, /device:TPU:0, one launch (start us, length us, event | category | flops | bytes accessed | tf_op | source)
XLA Modules:
  0.0 230.0 jit_solution(1138776864522754009)
XLA Ops:
  6.5 0.7 all-gather.8.cloned.1.call-update
  7.3 0.7 all-gather.10.cloned.1.call-update
  8.1 1.2 reshape.164
  10.2 1.1 reshape.163
  11.3 1.0 neg.24
  13.0 106.6 %while.46 = (s32[]{:T(128)}, f32[4,128,64]{1,2,0:T(8,128)S(1)}, f32[4,4,64,128]{3,2,1,0:T(8,128)}, f32[4,4,64,64]{3,1,2,0:T(4,128)}, f32[4,4,64,64]{3,1,2,0:T(4,...) while((s32[]{:T(128)}, f32[4,128,64]{1,2,0:T(8,128)S(1)}, ...), condition=%wide.region_10.11_spmd.clone.clone, body=%wide.region_8.10_spmd.clone.clone.sunk | while | flops 253308992 | bytes 5993869 | solution.py:175
  13.0 0.9 constant_dynamic-slice_fusion.20
  14.1 0.9 constant_dynamic-slice_fusion.19
  15.6 19.7 %custom-call.11 = f32[4,1,64,64]{2,3,1,0:T(8,128)S(1)} custom-call(f32[4,1,64,64]{3,2,1,0:T(8,128)S(1)} %fusion.172), custom_call_target="InvertDiagBlocksLowerTriangular" | custom-call | tf_op jit(solution)/shard_map/while/body/eval_jaxpr/jit(_solve_triangular)/vmap()/triangular_solve | solution.py:158
  37.9 0.9 fusion.176
  39.2 0.4 convolution_add_fusion.12
  39.6 0.9 constant_dynamic-slice_fusion.20
  40.7 0.9 constant_dynamic-slice_fusion.19
  42.2 19.7 %custom-call.11 = f32[4,1,64,64]{2,3,1,0:T(8,128)S(1)} custom-call(f32[4,1,64,64]{3,2,1,0:T(8,128)S(1)} %fusion.172), custom_call_target="InvertDiagBlocksLowerTriangular" | custom-call | tf_op jit(solution)/shard_map/while/body/eval_jaxpr/jit(_solve_triangular)/vmap()/triangular_solve | solution.py:158
  64.5 0.9 fusion.176
  65.9 0.4 convolution_add_fusion.12
  66.3 0.9 constant_dynamic-slice_fusion.20
  67.4 0.9 constant_dynamic-slice_fusion.19
  68.9 19.7 %custom-call.11 = f32[4,1,64,64]{2,3,1,0:T(8,128)S(1)} custom-call(f32[4,1,64,64]{3,2,1,0:T(8,128)S(1)} %fusion.172), custom_call_target="InvertDiagBlocksLowerTriangular" | custom-call | tf_op jit(solution)/shard_map/while/body/eval_jaxpr/jit(_solve_triangular)/vmap()/triangular_solve | solution.py:158
  91.2 0.9 fusion.176
  92.5 0.4 convolution_add_fusion.12
  92.9 0.9 constant_dynamic-slice_fusion.20
  94.0 0.9 constant_dynamic-slice_fusion.19
  95.5 19.7 %custom-call.11 = f32[4,1,64,64]{2,3,1,0:T(8,128)S(1)} custom-call(f32[4,1,64,64]{3,2,1,0:T(8,128)S(1)} %fusion.172), custom_call_target="InvertDiagBlocksLowerTriangular" | custom-call | tf_op jit(solution)/shard_map/while/body/eval_jaxpr/jit(_solve_triangular)/vmap()/triangular_solve | solution.py:158
  117.8 0.9 fusion.176
  119.2 0.4 convolution_add_fusion.12
  119.7 15.7 %all-gather.3 = bf16[16,64,64]{2,1,0:T(8,128)(2,1)S(1)} all-gather(bf16[4,64,64]{2,1,0:T(8,128)(2,1)S(1)} %get-tuple-element.533), channel_id=5, replica_groups=mesh['sp'=4,'fs'=4,'tp'=2] {'sp'}, dimensions={0}, use_global_device_ids=true | all-gather | bytes 163840 | tf_op jit(solution)/shard_map/all_gather | solution.py:16
  135.4 14.6 %all-gather.4 = bf16[16,64,64]{2,1,0:T(8,128)(2,1)S(1)} all-gather(bf16[4,64,64]{2,1,0:T(8,128)(2,1)S(1)} %get-tuple-element.532), channel_id=6, replica_groups=mesh['sp'=4,'fs'=4,'tp'=2] {'sp'}, dimensions={0}, use_global_device_ids=true | all-gather | bytes 163840 | tf_op jit(solution)/shard_map/all_gather | solution.py:16
  150.0 1.0 copy-done
  151.4 1.7 fusion.65
  153.7 0.8 copy.73
  154.9 0.8 copy.72
  156.0 13.2 %all-gather.1 = f32[1,1024,4]{1,2,0:T(4,128)S(1)} all-gather(f32[1,256,4]{1,2,0:T(4,128)S(1)} %copy-done.10), channel_id=3, replica_groups=mesh['sp'=4,'fs'=4,'tp'=2] {'sp'}, dimensions={1}, use_global_device_ids=true | all-gather | bytes 20480 | tf_op jit(solution)/shard_map/all_gather | solution.py:44
  169.2 14.5 %all-gather = bf16[1,1024,128]{1,2,0:T(8,128)(2,1)S(1)} all-gather(bf16[1,256,128]{1,2,0:T(8,128)(2,1)S(1)} %copy.55), channel_id=2, replica_groups=mesh['sp'=4,'fs'=4,'tp'=2] {'sp'}, dimensions={1}, use_global_device_ids=true | all-gather | bytes 327680 | tf_op jit(solution)/shard_map/all_gather | solution.py:53
  183.7 14.0 %all-gather.2 = bf16[1,1024,128]{1,2,0:T(8,128)(2,1)S(1)} all-gather(bf16[1,256,128]{1,2,0:T(8,128)(2,1)S(1)} %copy.56), channel_id=4, replica_groups=mesh['sp'=4,'fs'=4,'tp'=2] {'sp'}, dimensions={1}, use_global_device_ids=true | all-gather | bytes 327680 | tf_op jit(solution)/shard_map/all_gather | solution.py:54
  197.7 10.5 %conditional.1 = (f32[256,2,2]{0,2,1:T(2,128)}, f32[256,2,2,64]{0,3,2,1:T(8,128)}) conditional(s32[]{:T(128)} %convert_element_type.58, () %tuple.38, (s32[]{:T(128)}, s32[256]{0:T(256)S(1)}, bf16[1,256,256]{2,1,0:T(8,128)(2,1)S(1)}, bf16[1024,128]{0,1:T(8,128)(2,1)S(1)}, f32[1,256,4]{1,2,0:T(4,128)S(1)}, /*index=5*/f32[1024,4]{0,1:T(4,128)S(1)}, ...), branch_computations={%region_0.0_spmd, %region_1.6_spmd} | conditional | flops 140318464 | bytes 8662403 | solution.py:101
  197.7 0.8 copy.57
  198.5 9.7 %while.44 = (s32[]{:T(128)}, f32[256,2,2]{0,2,1:T(2,128)S(1)}, f32[256,2,2]{0,2,1:T(2,128)}, f32[256,2,2,64]{0,3,2,1:T(8,128)}, s32[256]{0:T(256)S(1)}, /*index=...) while((s32[]{:T(128)}, f32[256,2,2]{0,2,1:T(2,128)S(1)}, ...), condition=%wide.wide.region_5.5_spmd.clone, body=%wide.wide.region_2.4_spmd.clone.sunk | while | flops 140318208 | bytes 8373459 | solution.py:96
  198.7 1.6 fusion.181
  200.7 0.6 fusion.184
  201.4 1.2 fusion.185
  202.8 1.6 fusion.181
  204.8 1.3 fusion.184
  206.1 2.1 fusion.185
  208.2 1.1 multiply_reduce_fusion.2
  209.5 1.7 fusion.67
  211.2 2.7 %fusion.54 = bf16[256,2048]{1,0:T(8,128)(2,1)} fusion(f32[256,2048]{1,0:T(8,128)S(1)} %fusion.67, bf16[256,2048]{1,0:T(8,128)(2,1)} %all-gather.10.cloned.1.call-done, f32[256,256]{1,0:T(8,128)S(1)} %copy-done.1, f32[256,256]{1,0:T(8,128)S(1)} %reshape.160, f32[256,256]{1,0:T(8,128)S(1)} %copy-done.2, f32[256]{0:T(256)S(1)} %copy-done.13), kind=kOutput, calls=%fused_computation.87 | convolution fusion | flops 269746176 | bytes 4981760 | tf_op jit(solution)/shard_map/dot_general | solution.py:227
  213.9 9.5 %reduce-scatter.2.cloned.1.call-done = bf16[128,2048]{1,0:T(8,128)(2,1)} async-done(((bf16[256,2048]{1,0:T(8,128)(2,1)}), bf16[128,2048]{1,0:T(8,128)(2,1)}) %reduce-scatter.2.cloned.1.call-update) | async-done | bytes 524304 | tf_op jit(solution)/shard_map/reduce_scatter | solution.py:228
  (167 shorter events, 19.3 us)
Async XLA Ops:
  6.5 3.6 %copy-start.4 = (bf16[1,256,256]{2,1,0:T(8,128)(2,1)S(1)}, bf16[1,256,256]{2,1,0:T(8,128)(2,1)}, u32[]{:S(2)}) copy-start(bf16[1,256,256]{2,1,0:T(8,128)(2,1)} %param.29) | copy-start | bytes 393220
  6.5 202.9 %all-gather.8.cloned.1.call-start = ((), (), s32[]{:S(2)}) async-start(), calls=%async_computation.1 | async-start | bytes 1310720 | tf_op jit(solution)/shard_map/all_gather | solution.py:223
  7.3 4.0 %copy-start.3 = (f32[1,256,256]{2,1,0:T(8,128)S(1)}, f32[1,256,256]{2,1,0:T(8,128)}, u32[]{:S(2)}) copy-start(f32[1,256,256]{2,1,0:T(8,128)} %param.30) | copy-start | bytes 786436
  7.3 203.9 %all-gather.10.cloned.1.call-start = ((), (), s32[]{:S(2)}) async-start(), calls=%async_computation.2 | async-start | bytes 1310720 | tf_op jit(solution)/shard_map/all_gather | solution.py:224
  8.0 215.4 %reduce-scatter.2.cloned.1.call-start = ((), (), s32[]{:S(2)}) async-start(), calls=%async_computation.3 | async-start | bytes 1572864 | tf_op jit(solution)/shard_map/reduce_scatter | solution.py:228
  9.6 2.7 %copy-start.5 = (bf16[1,256,256]{2,1,0:T(8,128)(2,1)S(1)}, bf16[1,256,256]{2,1,0:T(8,128)(2,1)}, u32[]{:S(2)}) copy-start(bf16[1,256,256]{2,1,0:T(8,128)(2,1)} %param.28) | copy-start | bytes 393220
  9.7 2.9 %copy-start.6 = (bf16[1,256,256]{2,1,0:T(8,128)(2,1)S(1)}, bf16[1,256,256]{2,1,0:T(8,128)(2,1)}, u32[]{:S(2)}) copy-start(bf16[1,256,256]{2,1,0:T(8,128)(2,1)} %param.26) | copy-start | bytes 393220
  150.0 1.0 copy-start
  153.1 2.7 %copy-start.8 = (bf16[1,256,128]{2,1,0:T(8,128)(2,1)S(1)}, bf16[1,256,128]{2,1,0:T(8,128)(2,1)}, u32[]{:S(2)}) copy-start(bf16[1,256,128]{2,1,0:T(8,128)(2,1)} %param.22) | copy-start | bytes 196612
  153.1 2.8 %copy-start.9 = (bf16[1,256,128]{2,1,0:T(8,128)(2,1)S(1)}, bf16[1,256,128]{2,1,0:T(8,128)(2,1)}, u32[]{:S(2)}) copy-start(bf16[1,256,128]{2,1,0:T(8,128)(2,1)} %param.23) | copy-start | bytes 196612
  153.1 2.9 %copy-start.10 = (f32[1,256,4]{1,2,0:T(4,128)S(1)}, f32[1,256,4]{1,2,0:T(4,128)}, u32[]{:S(2)}) copy-start(f32[1,256,4]{1,2,0:T(4,128)} %param.24) | copy-start | bytes 12292
  153.4 44.3 %copy-start.7 = (bf16[1,256,256]{2,1,0:T(8,128)(2,1)S(1)}, bf16[1,256,256]{2,1,0:T(8,128)(2,1)}, u32[]{:S(2)}) copy-start(bf16[1,256,256]{2,1,0:T(8,128)(2,1)} %param.21) | copy-start | bytes 393220
  197.7 11.6 %copy-start.12 = (f32[256]{0:T(256)S(1)}, f32[256]{0:T(256)}, u32[]{:S(2)}) copy-start(f32[256]{0:T(256)} %param.25) | copy-start | bytes 3076
  197.7 0.8 copy-start.11
  208.2 3.0 %copy-start.1 = (f32[256,256]{1,0:T(8,128)S(1)}, f32[256,256]{1,0:T(8,128)}, u32[]{:S(2)}) copy-start(f32[256,256]{1,0:T(8,128)} %copy.73) | copy-start | bytes 786436
  208.2 3.0 %copy-start.2 = (f32[256,256]{1,0:T(8,128)S(1)}, f32[256,256]{1,0:T(8,128)}, u32[]{:S(2)}) copy-start(f32[256,256]{1,0:T(8,128)} %copy.72) | copy-start | bytes 786436
  208.2 3.0 %copy-start.13 = (f32[256]{0:T(256)S(1)}, f32[256]{0:T(256)}, u32[]{:S(2)}) copy-start(f32[256]{0:T(256)} %param.31) | copy-start | bytes 3076
Sparse Core Ops, SparseCore 0:
  9.2 29.8 all-gather.7
  40.9 27.0 all-gather.9
  214.0 9.3 reduce-scatter.1
where the time goes:
time: 231 us; the launch traced here: 230 us
  other arithmetic  85.3 us (37%)
  blocking collectives  71.9 us (31%)
  matrix products  30.9 us (13%)
  local copies, waits for them, and re-layouts  16.6 us (7%)
  between operations  13.5 us (6%)
  waiting for transfers between devices  11 us (5%)
    another operation x12, other arithmetic, one_span(): jax.scipy.linalg.solve_triangular(identity_span - mix_erase, right_side,...  79 us
    all_gather x2, blocking collectives, carried_in(): lax.all_gather(a.astype(kind), axis)  30.2 us
    dot_general x44, matrix products, product(): return jnp.einsum(form, left, right, precision=HIGHEST)  16.7 us
    all_gather x1, blocking collectives, forget_attention(): key_piece = lax.all_gather(key_rows, 'sp', axis=0, tiled=True)  14.5 us
    all_gather x1, blocking collectives, forget_attention(): value_piece = lax.all_gather(value_rows, 'sp', axis=0, tiled=True)  14 us
    all_gather x1, blocking collectives, forget_attention(): forget_all = lax.all_gather(forget_rows, 'sp', axis=0, tiled=True)  13.2 us
    reduce_scatter x1, waiting for transfers between devices, shards(): lax.psum_scatter(round_half(partial_value).astype(jnp.bfloat16), 'tp', sc...  9.53 us
    dynamic_slice x20, local copies, waits for them, and re-layouts, delta_attention(): lax.scan(one_span, start_state, (recept, key_float, value_float, unit_key...  7.59 us
  transfers between devices with their start and end apart: 3, of which 1 were waited for; matrix products, arithmetic and copies ran while one was open for 56% of the time, Pallas kernels for 0%

commit v1 on v0

--- a/solution.py
+++ b/solution.py
@@ -51,7 +51,12 @@
         jnp.zeros((row_count, kv_count, group_size, HEAD), jnp.float32),
     )
     key_piece = lax.all_gather(key_rows, "sp", axis=0, tiled=True)
-    value_piece = lax.all_gather(value_rows, "sp", axis=0, tiled=True)
+    ring = [value_rows]
+    for hop in range(3):
+        ring.append(lax.ppermute(ring[-1], "sp", [(dev, (dev + 1) % 4) for dev in range(4)]))
+    value_piece = jnp.roll(
+        jnp.concatenate(ring[::-1], axis=0), (lax.axis_index("sp") + 1) * ring[0].shape[0], axis=0
+    )
     piece_rows = key_piece.shape[0]
     block_rows = math.gcd(piece_rows, 512)
 

time: 231 us -> 225 us (0.974)
  blocking collectives: 71.9 us -> 56.2 us
  starting transfers between devices: 0.08 us -> 4.86 us
  local copies, waits for them, and re-layouts: 16.6 us -> 20.6 us
  other arithmetic: 85.3 us -> 87.7 us
    all_gather x1 -> x0, blocking collectives: 14 us -> none  [forget_attention(): value_piece = lax.all_gather(value_rows, 'sp', axis=0, tiled=True)]
    ppermute x0 -> x3, starting transfers between devices: none -> 4.78 us  [forget_attention(): lax.ppermute(ring[-1], 'sp', [(dev, (dev + 1) % 4) for dev in range(4)])]
    unnamed x28 -> x33, local copies, waits for them, and re-layouts: 1.29 us -> 3.84 us
  transfers between devices with their start and end apart: 3 -> 6, of which waited for: 1 -> 1; matrix products, arithmetic and copies ran while one was open for 56% -> 60% of each run, Pallas kernels for 0% -> 0%
where the time goes in v1:
time: 225 us; the launch traced here: 224 us
  other arithmetic  87.7 us (39%)
  blocking collectives  56.2 us (25%)
  matrix products  30.9 us (14%)
  local copies, waits for them, and re-layouts  20.6 us (9%)
  between operations  13.5 us (6%)
  waiting for transfers between devices  9.96 us (4%)
  starting transfers between devices  4.86 us (2%)
    another operation x12, other arithmetic, one_span(): jax.scipy.linalg.solve_triangular(identity_span - mix_erase, right_side,...  79 us
    all_gather x2, blocking collectives, carried_in(): lax.all_gather(a.astype(kind), axis)  27.9 us
    dot_general x44, matrix products, product(): return jnp.einsum(form, left, right, precision=HIGHEST)  16.7 us
    all_gather x1, blocking collectives, forget_attention(): forget_all = lax.all_gather(forget_rows, 'sp', axis=0, tiled=True)  14.3 us
    all_gather x1, blocking collectives, forget_attention(): key_piece = lax.all_gather(key_rows, 'sp', axis=0, tiled=True)  14 us
    reduce_scatter x1, waiting for transfers between devices, shards(): lax.psum_scatter(round_half(partial_value).astype(jnp.bfloat16), 'tp', sc...  9.17 us
    dynamic_slice x20, local copies, waits for them, and re-layouts, delta_attention(): lax.scan(one_span, start_state, (recept, key_float, value_float, unit_key...  7.59 us
    ppermute x3, starting transfers between devices, forget_attention(): lax.ppermute(ring[-1], 'sp', [(dev, (dev + 1) % 4) for dev in range(4)])  4.78 us
  transfers between devices with their start and end apart: 6, of which 1 were waited for; matrix products, arithmetic and copies ran while one was open for 60% of the time, Pallas kernels for 0%

profile of v1, /device:TPU:0, one launch (start us, length us, event | category | flops | bytes accessed | tf_op | source)
XLA Modules:
  0.0 224.4 jit_solution(11633914125357268364)
XLA Ops:
  6.5 0.7 all-gather.7.cloned.1.call-update
  7.3 0.9 copy.56
  8.3 3.1 %collective-permute-start = (bf16[256,128]{0,1:T(8,128)(2,1)S(1)}, bf16[256,128]{0,1:T(8,128)(2,1)}, u32[]{:S(2)}, u32[]{:S(2)}) collective-permute-start(bf16[256,128]{0,1:T(8,128)(2,1)S(1)} %bitcast.239), channel_id=1, source_target_pairs={{0,8},{8,16},{16,24},{24,0},{1,9},{9,17},{17,25},{25,1},{2,10},{10... | collective-permute-start | bytes 196616 | tf_op jit(solution)/shard_map/ppermute | solution.py:56
  11.5 1.2 reshape.164
  13.6 1.0 reshape.163
  14.7 1.1 neg.24
  16.4 106.6 %while.56 = (s32[]{:T(128)}, f32[4,128,64]{1,2,0:T(8,128)S(1)}, f32[4,4,64,128]{3,2,1,0:T(8,128)}, f32[4,4,64,64]{3,1,2,0:T(4,128)}, f32[4,4,64,64]{3,1,2,0:T(4,...) while((s32[]{:T(128)}, f32[4,128,64]{1,2,0:T(8,128)S(1)}, ...), condition=%wide.region_10.11_spmd.clone.clone, body=%wide.region_8.10_spmd.clone.clone.sunk | while | flops 253308992 | bytes 5993869 | solution.py:180
  16.4 0.9 constant_dynamic-slice_fusion.21
  17.5 0.9 constant_dynamic-slice_fusion.20
  19.0 19.7 %custom-call.13 = f32[4,1,64,64]{2,3,1,0:T(8,128)S(1)} custom-call(f32[4,1,64,64]{3,2,1,0:T(8,128)S(1)} %fusion.172), custom_call_target="InvertDiagBlocksLowerTriangular" | custom-call | tf_op jit(solution)/shard_map/while/body/eval_jaxpr/jit(_solve_triangular)/vmap()/triangular_solve | solution.py:163
  41.3 0.9 fusion.176
  43.0 0.9 constant_dynamic-slice_fusion.21
  44.1 0.9 constant_dynamic-slice_fusion.20
  45.6 19.7 %custom-call.13 = f32[4,1,64,64]{2,3,1,0:T(8,128)S(1)} custom-call(f32[4,1,64,64]{3,2,1,0:T(8,128)S(1)} %fusion.172), custom_call_target="InvertDiagBlocksLowerTriangular" | custom-call | tf_op jit(solution)/shard_map/while/body/eval_jaxpr/jit(_solve_triangular)/vmap()/triangular_solve | solution.py:163
  67.9 0.9 fusion.176
  69.7 0.9 constant_dynamic-slice_fusion.21
  70.8 0.9 constant_dynamic-slice_fusion.20
  72.3 19.7 %custom-call.13 = f32[4,1,64,64]{2,3,1,0:T(8,128)S(1)} custom-call(f32[4,1,64,64]{3,2,1,0:T(8,128)S(1)} %fusion.172), custom_call_target="InvertDiagBlocksLowerTriangular" | custom-call | tf_op jit(solution)/shard_map/while/body/eval_jaxpr/jit(_solve_triangular)/vmap()/triangular_solve | solution.py:163
  94.6 0.9 fusion.176
  96.3 0.9 constant_dynamic-slice_fusion.21
  97.4 0.9 constant_dynamic-slice_fusion.20
  98.9 19.7 %custom-call.13 = f32[4,1,64,64]{2,3,1,0:T(8,128)S(1)} custom-call(f32[4,1,64,64]{3,2,1,0:T(8,128)S(1)} %fusion.172), custom_call_target="InvertDiagBlocksLowerTriangular" | custom-call | tf_op jit(solution)/shard_map/while/body/eval_jaxpr/jit(_solve_triangular)/vmap()/triangular_solve | solution.py:163
  121.2 0.9 fusion.176
  123.1 14.2 %all-gather.2 = bf16[16,64,64]{2,1,0:T(8,128)(2,1)S(1)} all-gather(bf16[4,64,64]{2,1,0:T(8,128)(2,1)S(1)} %get-tuple-element.682), channel_id=4, replica_groups=mesh['sp'=4,'fs'=4,'tp'=2] {'sp'}, dimensions={0}, use_global_device_ids=true | all-gather | bytes 163840 | tf_op jit(solution)/shard_map/all_gather | solution.py:16
  137.3 13.8 %all-gather.3 = bf16[16,64,64]{2,1,0:T(8,128)(2,1)S(1)} all-gather(bf16[4,64,64]{2,1,0:T(8,128)(2,1)S(1)} %get-tuple-element.681), channel_id=5, replica_groups=mesh['sp'=4,'fs'=4,'tp'=2] {'sp'}, dimensions={0}, use_global_device_ids=true | all-gather | bytes 163840 | tf_op jit(solution)/shard_map/all_gather | solution.py:16
  151.1 1.0 copy-done
  152.5 1.7 fusion.65
  155.7 0.8 copy.73
  156.5 14.3 %all-gather.1 = f32[1,1024,4]{1,2,0:T(4,128)} all-gather(f32[1,256,4]{1,2,0:T(4,128)S(1)} %copy-done.10), channel_id=3, replica_groups=mesh['sp'=4,'fs'=4,'tp'=2] {'sp'}, dimensions={1}, use_global_device_ids=true | all-gather | bytes 20480 | tf_op jit(solution)/shard_map/all_gather | solution.py:44
  170.8 1.4 collective-permute-start.2
  172.2 14.0 %all-gather = bf16[1,1024,128]{1,2,0:T(8,128)(2,1)S(1)} all-gather(bf16[1,256,128]{1,2,0:T(8,128)(2,1)S(1)} %copy.57), channel_id=2, replica_groups=mesh['sp'=4,'fs'=4,'tp'=2] {'sp'}, dimensions={1}, use_global_device_ids=true | all-gather | bytes 327680 | tf_op jit(solution)/shard_map/all_gather | solution.py:53
  186.2 0.8 constant_dynamic-update-slice_fusion.5
  187.1 0.8 constant_dynamic-update-slice_fusion.1
  188.0 14.4 %conditional.1 = (f32[256,2,2]{0,2,1:T(2,128)}, f32[256,2,2,64]{0,3,2,1:T(8,128)}) conditional(s32[]{:T(128)} %convert_element_type.58, () %tuple.52, (s32[]{:T(128)}, s32[]{:T(128)}, bf16[2048,128]{0,1:T(8,128)(2,1)S(1)}, s32[]{:T(128)}, s32[256]{0:T(256)S(1)}, /*index=5*/bf16[1,256,256]{2,1,0:T(8,128)(2,1)S(1)}, ...), branch_computations={%region_0.1_spmd, %region_1.6_spmd.clone} | conditional | flops 140318480 | bytes 9186850 | solution.py:106
  188.8 0.7 copy.58
  190.1 12.3 %while.54 = (s32[]{:T(128)}, f32[256,2,2]{0,2,1:T(2,128)S(1)}, f32[256,2,2]{0,2,1:T(2,128)}, f32[256,2,2,64]{0,3,2,1:T(8,128)}, s32[256]{0:T(256)}, /*index=5*/b...) while((s32[]{:T(128)}, f32[256,2,2]{0,2,1:T(2,128)S(1)}, ...), condition=%wide.wide.region_5.5_spmd.clone, body=%wide.wide.region_2.4_spmd.clone.sunk | while | flops 140318208 | bytes 8373459 | solution.py:101
  190.8 0.8 broadcast_compare_fusion.3
  191.6 1.6 fusion.181
  194.2 1.2 fusion.185
  196.2 0.8 broadcast_compare_fusion.3
  196.9 1.6 fusion.181
  198.9 1.3 fusion.184
  200.2 2.1 fusion.185
  202.4 1.0 multiply_reduce_fusion.2
  203.4 0.8 fusion.59
  204.3 1.7 fusion.67
  206.0 2.7 %fusion.54 = bf16[256,2048]{1,0:T(8,128)(2,1)} fusion(f32[256,2048]{1,0:T(8,128)S(1)} %fusion.67, bf16[256,2048]{1,0:T(8,128)(2,1)} %all-gather.9.cloned.1.call-done, f32[256,256]{1,0:T(8,128)S(1)} %copy.74, f32[256,256]{1,0:T(8,128)S(1)} %reshape.160, f32[256,256]{1,0:T(8,128)S(1)} %copy-done.1, f32[256]{0:T(256)S(1)} %copy-done.12), kind=kOutput, calls=%fused_computation.88 | convolution fusion | flops 269746176 | bytes 4981760 | tf_op jit(solution)/shard_map/dot_general | solution.py:232
  208.7 9.2 %reduce-scatter.2.cloned.1.call-done = bf16[128,2048]{1,0:T(8,128)(2,1)} async-done(((bf16[256,2048]{1,0:T(8,128)(2,1)}), bf16[128,2048]{1,0:T(8,128)(2,1)}) %reduce-scatter.2.cloned.1.call-update) | async-done | bytes 524304 | tf_op jit(solution)/shard_map/reduce_scatter | solution.py:233
  (179 shorter events, 24.1 us)
Async XLA Ops:
  6.5 6.9 %copy-start.5 = (bf16[1,256,256]{2,1,0:T(8,128)(2,1)S(1)}, bf16[1,256,256]{2,1,0:T(8,128)(2,1)}, u32[]{:S(2)}) copy-start(bf16[1,256,256]{2,1,0:T(8,128)(2,1)} %param.29) | copy-start | bytes 393220
  6.5 197.7 %all-gather.7.cloned.1.call-start = ((), (), s32[]{:S(2)}) async-start(), calls=%async_computation.1 | async-start | bytes 1310720 | tf_op jit(solution)/shard_map/all_gather | solution.py:228
  7.3 198.7 %all-gather.9.cloned.1.call-start = ((), (), s32[]{:S(2)}) async-start(), calls=%async_computation.2 | async-start | bytes 1310720 | tf_op jit(solution)/shard_map/all_gather | solution.py:229
  8.2 6.4 %copy-start.2 = (bf16[1,256,128]{1,2,0:T(8,128)(2,1)}, bf16[1,256,128]{1,2,0:T(8,128)(2,1)S(1)}, u32[]{:S(2)}) copy-start(bf16[1,256,128]{1,2,0:T(8,128)(2,1)S(1)} %copy.56) | copy-start | bytes 196612
  8.3 6.4 %copy-start.4 = (f32[1,256,256]{2,1,0:T(8,128)S(1)}, f32[1,256,256]{2,1,0:T(8,128)}, u32[]{:S(2)}) copy-start(f32[1,256,256]{2,1,0:T(8,128)} %param.30) | copy-start | bytes 786436
  8.3 146.1 %collective-permute-start = (bf16[256,128]{0,1:T(8,128)(2,1)S(1)}, bf16[256,128]{0,1:T(8,128)(2,1)}, u32[]{:S(2)}, u32[]{:S(2)}) collective-permute-start(bf16[256,128]{0,1:T(8,128)(2,1)S(1)} %bitcast.239), channel_id=1, source_target_pairs={{0,8},{8,16},{16,24},{24,0},{1,9},{9,17},{17,25},{25,1},{2,10},{10... | collective-permute-start | bytes 196616 | tf_op jit(solution)/shard_map/ppermute | solution.py:56
  11.4 206.4 %reduce-scatter.2.cloned.1.call-start = ((), (), s32[]{:S(2)}) async-start(), calls=%async_computation.3 | async-start | bytes 1572864 | tf_op jit(solution)/shard_map/reduce_scatter | solution.py:233
  13.0 2.7 %copy-start.6 = (bf16[1,256,256]{2,1,0:T(8,128)(2,1)S(1)}, bf16[1,256,256]{2,1,0:T(8,128)(2,1)}, u32[]{:S(2)}) copy-start(bf16[1,256,256]{2,1,0:T(8,128)(2,1)} %param.28) | copy-start | bytes 393220
  13.0 2.9 %copy-start.7 = (bf16[1,256,256]{2,1,0:T(8,128)(2,1)S(1)}, bf16[1,256,256]{2,1,0:T(8,128)(2,1)}, u32[]{:S(2)}) copy-start(bf16[1,256,256]{2,1,0:T(8,128)(2,1)} %param.26) | copy-start | bytes 393220
  151.1 1.0 copy-start
  152.1 2.8 %copy-start.9 = (bf16[1,256,128]{2,1,0:T(8,128)(2,1)S(1)}, bf16[1,256,128]{2,1,0:T(8,128)(2,1)}, u32[]{:S(2)}) copy-start(bf16[1,256,128]{2,1,0:T(8,128)(2,1)} %param.22) | copy-start | bytes 196612
  154.2 2.3 %copy-start.10 = (f32[1,256,4]{1,2,0:T(4,128)S(1)}, f32[1,256,4]{1,2,0:T(4,128)}, u32[]{:S(2)}) copy-start(f32[1,256,4]{1,2,0:T(4,128)} %param.24) | copy-start | bytes 12292
  154.3 16.5 %collective-permute-start.1 = (bf16[256,128]{0,1:T(8,128)(2,1)}, bf16[256,128]{0,1:T(8,128)(2,1)S(1)}, u32[]{:S(2)}, u32[]{:S(2)}) collective-permute-start(bf16[256,128]{0,1:T(8,128)(2,1)} %collective-permute-done), channel_id=1, source_target_pairs={{0,8},{8,16},{16,24},{24,0},{1,9},{9,17},{17,25},{25,1},{2,10},{10... | collective-permute-start | bytes 196616 | tf_op jit(solution)/shard_map/ppermute | solution.py:56
  154.6 32.5 %copy-start.3 = (bf16[1,256,128]{1,2,0:T(8,128)(2,1)S(1)}, bf16[1,256,128]{1,2,0:T(8,128)(2,1)}, u32[]{:S(2)}) copy-start(bf16[1,256,128]{1,2,0:T(8,128)(2,1)} %copy-done.2) | copy-start | bytes 196612
  154.8 33.2 %copy-start.8 = (bf16[1,256,256]{2,1,0:T(8,128)(2,1)S(1)}, bf16[1,256,256]{2,1,0:T(8,128)(2,1)}, u32[]{:S(2)}) copy-start(bf16[1,256,256]{2,1,0:T(8,128)(2,1)} %param.21) | copy-start | bytes 393220
  170.8 15.4 %collective-permute-start.2 = (bf16[256,128]{0,1:T(8,128)(2,1)S(1)}, bf16[256,128]{0,1:T(8,128)(2,1)S(1)}, u32[]{:S(2)}, u32[]{:S(2)}) collective-permute-start(bf16[256,128]{0,1:T(8,128)(2,1)S(1)} %collective-permute-done.1), channel_id=1, source_target_pairs={{0,8},{8,16},{16,24},{24,0},{1,9},{9,17},{17,25},{25,1},{2,10},{10... | collective-permute-start | bytes 196616 | tf_op jit(solution)/shard_map/ppermute | solution.py:56
  188.0 2.1 copy-start.11
  202.4 3.6 %copy-start.1 = (f32[256,256]{1,0:T(8,128)S(1)}, f32[256,256]{1,0:T(8,128)}, u32[]{:S(2)}) copy-start(f32[256,256]{1,0:T(8,128)} %copy.73) | copy-start | bytes 786436
  202.4 3.6 %copy-start.12 = (f32[256]{0:T(256)S(1)}, f32[256]{0:T(256)}, u32[]{:S(2)}) copy-start(f32[256]{0:T(256)} %param.31) | copy-start | bytes 3076
Sparse Core Ops, SparseCore 0:
  9.2 30.1 all-gather.6
  41.1 26.5 all-gather.8
  208.8 8.9 reduce-scatter.1
